TPU v7x, 512 devices: a 4x2x32 block of a 4x8x32 slice. The times are simulated.
512 devices in a mesh: grp: 2 (over y), fs: 64 (over z, core), tp: 4 (over x).
Axes of the slice: x: 4, y: 2, z: 32, core: 2. Of those that a mesh axis runs over, the one named last changes fastest.
The devices are a block of a 4x8x32 slice.
Arguments:
- tokens: bfloat16 [2048, 3072], P(('grp', 'tp')), parts along dimension 0, may hold values from -6 to 6
- up_master: float32 [3072, 12288], P('fs', 'tp'), may hold values from -0.109375 to 0.109375
- down_master: float32 [12288, 3072], P('fs', 'tp'), may hold values from -0.0546875 to 0.0546875
- norm_gain: float32 [3072], P('fs'), may hold values from 0.1 to 1.9
Outputs:
- prompt_out: bfloat16 [2048, 3072], P(('grp', 'tp'), 'fs'), parts along dimension 0
- sampled_up: bfloat16 [6144, 12288], P('grp', 'fs'), parts along dimension 0
- sampled_down: bfloat16 [24576, 3072], P(('grp', 'fs')), parts along dimension 0
There are 2 independent parts, one for each index of `grp`. A program takes and returns all parts, laid end to end along the dimension named above; an argument that names none is the same for every part. Nothing has to cross between parts.
All inputs are finite; a program needn't handle non-finite values.
Results may differ from a plain program's by a relative error of at most 0.0074.
Values may be sent and summed in bfloat16 or wider, within the bound.
A program may use at most 64 MiB of HBM per device.

v0:
```python
import functools

import jax
import jax.numpy as jnp
from jax import lax
from jax.experimental import pallas as pl
from jax.experimental.pallas import tpu as pltpu
from jax.sharding import PartitionSpec as P

MESH = pl.DeviceIdType.MESH
BF16 = jnp.bfloat16
F32 = jnp.float32


def kernel(
    nz, nx, tok_hbm, upm_hbm, dnm_hbm, gain_hbm, out_ref, upt_ref, dn_ref,
    tok, upm, dnm, gain, stage, slots, up, dn, nrm, dnt, upt, acc, ht, terms, rs_out, rs_in, outb,
    in_sem, xa_send, xa_recv, dy_send, dy_recv, zs_send, zs_recv, y_send, y_recv, x_send, x_recv, dn_send, dn_recv,
    rs_send, rs_recv, o_send, o_recv, l_sem,
):
    g, fs, x = lax.axis_index("grp"), lax.axis_index("fs"), lax.axis_index("tp")
    z, c = fs // 2, fs % 2
    par = g % 2
    other = g + 1 - 2 * par
    main = c == par
    agent = c != par
    adds = c == 1
    apart = jnp.logical_and(main, c == 0)
    right, left = (x + 1) % nx, (x + nx - 1) % nx
    per_col = nz // nx
    quarter = z // per_col
    shift = (nx - 1) - z % nx
    served = (x + nx - shift) % nx
    residue = (2 * nx - 1 - x + quarter) % nx
    far = (x + 2) % nx
    half = nz // 2
    rows = upm.shape[0]
    hid = dnm.shape[0]
    dcols = dnm.shape[1]
    wide = 2 * hid
    feat = 2 * rows

    def dev(g_, z_, c_, x_):
        return {"grp": g_, "fs": 2 * z_ + c_, "tp": x_}

    def remote(src, dst, ssem, rsem, to):
        return pltpu.make_async_remote_copy(
            src_ref=src, dst_ref=dst, send_sem=ssem, recv_sem=rsem, device_id=to, device_id_type=MESH
        )

    def up_rows(zs, cs):
        return up.at[pl.ds(pl.multiple_of((2 * zs + cs) * rows, 16), rows), :]

    def dn_part(h, xs):
        return dn.at[pl.ds(h * hid, hid), pl.ds(pl.multiple_of(xs * dcols, 128), dcols)]

    loads = [
        pltpu.make_async_copy(upm_hbm, upm, in_sem.at[0]),
        pltpu.make_async_copy(gain_hbm, gain, in_sem.at[1]),
        pltpu.make_async_copy(dnm_hbm, dnm, in_sem.at[2]),
        pltpu.make_async_copy(tok_hbm, tok, in_sem.at[3]),
    ]
    for k in range(4):
        loads[k].start()

    barrier = pltpu.get_barrier_semaphore()

    def greet(to):
        pl.semaphore_signal(barrier, inc=1, device_id=to, device_id_type=MESH)

    @pl.when(main)
    def _():
        def greet_agent(i, carry):
            greet(dev(g, i * nx + residue, 1 - par, x))
            return carry

        lax.fori_loop(0, per_col, greet_agent, 0)
        for to_x in (right, left):
            greet(dev(g, z, par, to_x))
        greet(dev(g, z, 1 - par, x))
        greet(dev(other, z, 1 - par, x))

    @pl.when(agent)
    def _():
        greet(dev(g, z, par, x))
        greet(dev(g, z, par, served))

    @pl.when(adds)
    def _():
        for d in (1, 2, nz - 1, nz - 2):
            greet(dev(g, (z + d) % nz, 1, x))

    loads[0].wait()
    loads[1].wait()

    @pl.when(main)
    def _():
        eye = lax.broadcasted_iota(jnp.int32, (rows, rows), 0) == lax.broadcasted_iota(jnp.int32, (rows, rows), 1)
        scale = jnp.sum(jnp.where(eye, gain[...], 0.0), axis=1, keepdims=True)
        stage[...] = (scale * upm[...]).astype(BF16)

    loads[2].wait()

    @pl.when(main)
    def _():
        dn_part(par, x)[...] = dnm[...].astype(BF16)

    peers = jnp.where(main, 5, 1 + per_col) + jnp.where(adds, 4, 0)
    pl.semaphore_wait(barrier, peers)

    rows_copy = remote(stage, slots, xa_send.at[0], xa_recv.at[0], dev(g, z, 1 - par, (x + shift) % nx))

    @pl.when(main)
    def _():
        rows_copy.start()

    def scatter_copy(j):
        part = slots.at[:, pl.ds(pl.multiple_of(j * wide, 128), wide)]
        return remote(
            part, up_rows(z, par), zs_send.at[j], zs_recv.at[z // nx], dev(g, per_col * served + j, par, x)
        )

    @pl.when(agent)
    def _():
        rows_copy.wait_recv()

        def scatter(k, carry):
            scatter_copy(k).start()
            return carry

        lax.fori_loop(0, per_col, scatter, 0)

    def to_mate(src, dst, k):
        return remote(src, dst, o_send.at[k], o_recv.at[k], dev(g, z, 1 - c, x))

    def half_of(ref, core, size):
        return ref.at[pl.ds(pl.multiple_of(core * size, 16), size), :]

    up_copy = to_mate(half_of(upt, 1 - par, hid), upt_ref, 0)
    dn_copy = to_mate(half_of(dn, 1 - par, hid), dn_ref, 1)
    out_copy = to_mate(outb.at[pl.ds(0, rows), :], out_ref, 2)
    dnt_copy = to_mate(dnt, dnt, 3)
    ht_copy = to_mate(ht, ht, 4)

    part_rows = hid // 2

    def down_part(xs, k):
        first = pl.multiple_of(par * hid + k * part_rows, 16)
        return dn.at[pl.ds(first, part_rows), pl.ds(pl.multiple_of(xs * dcols, 128), dcols)]

    def down_copy(xs, k, d, relayed):
        part = down_part(xs, k)
        return remote(
            part, part, dn_send.at[d, k, relayed], dn_recv.at[d, k, relayed], dev(g, z, par, left if d else right)
        )

    def down_across(xs, k, mine):
        part = dn_part(par if mine else 1 - par, xs)
        return remote(part, part, dy_send.at[k], dy_recv.at[k], dev(other, z, 1 - par, x))

    def piece(xs, k, i):
        cs = par if k == 0 else 1 - par
        return up_rows(nx * i + (2 * nx - 1 - xs + quarter) % nx, cs)

    def x_copy(xs, k, i, slot, to_right):
        d = 0 if to_right else 1
        part = piece(xs, k, i)
        return remote(part, part, x_send.at[d, slot], x_recv.at[d, slot], dev(g, z, par, right if to_right else left))

    def y_copy(i, mine):
        part = piece(x, 0 if mine else 1, i)
        return remote(part, part, y_send.at[i], y_recv.at[i], dev(other, z, 1 - par, x))

    def relay_slot(k, i):
        return 2 * per_col + k * (per_col // 2) + i // 2

    def relay(k, i):

        @pl.when(i % 2 == 0)
        def _():
            x_copy(left, k, i, k * per_col + i, True).wait_recv()
            x_copy(left, k, i, relay_slot(k, i), True).start()

        @pl.when(i % 2 == 1)
        def _():
            x_copy(right, k, i, k * per_col + i, False).wait_recv()
            x_copy(right, k, i, relay_slot(k, i), False).start()

    @pl.when(main)
    def _():
        for k in range(2):
            down_copy(x, k, 0, 0).start()
            down_copy(x, 1 - k, 1, 0).start()
        down_across(x, 0, True).start()

        loads[3].wait()
        block = 64

        def norm(b, carry):
            sl = pl.ds(pl.multiple_of(b * block, block), block)
            values = tok[sl, :].astype(F32)
            center = jnp.mean(values, axis=-1, keepdims=True)
            spread = jnp.mean(jnp.square(values - center), axis=-1, keepdims=True)
            nrm[sl, :] = ((values - center) * lax.rsqrt(spread + 1e-05)).astype(BF16)
            return carry

        lax.fori_loop(0, tok.shape[0] // block, norm, 0)

        down_copy(left, 0, 0, 0).wait_recv()
        down_copy(left, 0, 0, 1).start()
        down_copy(right, 1, 1, 0).wait_recv()
        down_copy(right, 1, 1, 1).start()
        down_copy(left, 1, 0, 0).wait_recv()
        down_across(left, 1, True).start()
        down_copy(right, 0, 1, 0).wait_recv()
        down_across(right, 2, True).start()

        def turn_down(j, carry):
            sl = pl.ds(pl.multiple_of(j * 128, 128), 128)
            dnt[sl, :] = dn[:, sl].T
            return carry

        own_dn = pltpu.make_async_copy(half_of(dn, par, hid), dn_ref, l_sem.at[0])

        def ordered(s):
            near_first = jnp.where(s % 2 == 0, per_col - 1 - s // 2, s // 2)
            return jnp.where(quarter == nx - 1, near_first, (s + 1) % per_col)

        chunk = nx * feat
        acc[...] = jnp.zeros_like(acc)

        def at_lag(s, lag, run):
            @pl.when(jnp.logical_and(s >= lag, s < per_col + lag))
            def _():
                run(ordered(s - lag))

        def arrived(i):
            remote(piece(x, 0, i), piece(x, 0, i), y_send.at[0], zs_recv.at[i], dev(other, z, 1 - par, x)).wait_recv()
            y_copy(i, True).start()
            x_copy(x, 0, i, i, True).start()
            x_copy(x, 0, i, i, False).start()

        def crossed(i):
            y_copy(i, False).wait_recv()
            x_copy(x, 1, i, per_col + i, True).start()
            x_copy(x, 1, i, per_col + i, False).start()
            relay(0, i)

        def complete(i):
            for k in range(2):

                @pl.when(i % 2 == 1)
                def _():
                    x_copy(left, k, i, k * per_col + i, True).wait_recv()
                    x_copy(far, k, i, relay_slot(k, i), False).wait_recv()

                @pl.when(i % 2 == 0)
                def _():
                    x_copy(right, k, i, k * per_col + i, False).wait_recv()
                    x_copy(far, k, i, relay_slot(k, i), True).wait_recv()

            sl = pl.ds(pl.multiple_of(i * chunk, 128), chunk)
            acc[...] += jnp.dot(nrm[:, sl], up[sl, :], preferred_element_type=F32)

        def gather_up(s, carry):
            @pl.when(s == 1)
            def _():
                down_copy(far, 0, 0, 1).wait_recv()
                down_copy(far, 1, 1, 1).wait_recv()
                down_across(far, 3, True).start()

            at_lag(s, 0, arrived)
            at_lag(s, 2, crossed)
            at_lag(s, 4, lambda i: relay(1, i))

            @pl.when(s == per_col)
            def _():
                for k, xs in enumerate((x, left, right, far)):
                    down_across(xs, k, False).wait_recv()
                own_dn.start()
                dn_copy.start()
                lax.fori_loop(0, dn.shape[1] // 128, turn_down, 0)

                @pl.when(apart)
                def _():
                    dnt_copy.start()

            at_lag(s, 5, complete)
            return carry

        lax.fori_loop(0, per_col + 5, gather_up, 0)

        ht[...] = jnp.square(jnp.maximum(acc[...], 0.0)).T.astype(BF16)

        @pl.when(apart)
        def _():
            ht_copy.start()

    def turn_up(j, carry):
        sl = pl.ds(pl.multiple_of(j * 128, 128), 128)
        upt[:, sl] = up[sl, :].T
        return carry

    turns = up.shape[0] // 128
    own_up = pltpu.make_async_copy(half_of(upt, par, hid), upt_ref, l_sem.at[1])
    own_out = pltpu.make_async_copy(outb.at[pl.ds(rows, rows), :], out_ref, l_sem.at[2])

    @pl.when(apart)
    def _():
        lax.fori_loop(0, turns, turn_up, 0)
        up_copy.start()
        own_up.start()

    @pl.when(jnp.logical_and(agent, adds))
    def _():
        dnt_copy.wait_recv()
        ht_copy.wait_recv()

    @pl.when(adds)
    def _():
        chains = ((1, 0), (1, 1), (-1, 1), (-1, 0))

        def rs_copy(ch, s, sub, dist):
            sign = chains[ch][0]
            to = (z + nz + sign * dist) % nz
            return remote(
                rs_out.at[ch, s, sub], rs_in.at[ch, s, sub], rs_send.at[ch, s, sub], rs_recv.at[ch, s, sub], dev(g, to, 1, x)
            )

        def rows_of(zt, sub):
            return pl.ds(pl.multiple_of(zt * feat + sub * rows, 16), rows)

        def step(s, skip, first_of):
            for sub in range(2):
                for ch in (1, 2, 0, 3):
                    if ch in skip:
                        continue
                    sign, odd = chains[ch]
                    d = half - odd - 2 * s
                    sl = rows_of((z + 2 * nz + sign * d) % nz, sub)
                    if isinstance(s, int) and s == 0:
                        value = jnp.dot(dnt[sl, :], ht[...], preferred_element_type=F32)
                    else:
                        value = terms[sl, :]
                    if ch not in first_of:
                        rs_copy(ch, s - 1, sub, 2).wait_recv()
                        value = value + rs_in[ch, s - 1, sub].astype(F32)
                    rs_out[ch, s, sub] = value.astype(BF16)
                    rs_copy(ch, s, sub, jnp.minimum(d, 2)).start()

        def turn_some(s):
            @pl.when(main)
            def _():
                lax.fori_loop(4 * s, jnp.minimum(4 * s + 4, turns), turn_up, 0)

        tc = 512

        def all_terms(b, carry):
            sl = pl.ds(pl.multiple_of(b * tc, tc), tc)
            terms[sl, :] = jnp.dot(dnt[sl, :], ht[...], preferred_element_type=F32)
            return carry

        steps = half // 2
        step(0, (3,), (0, 1, 2))
        lax.fori_loop(0, terms.shape[0] // tc, all_terms, 0)
        turn_some(0)
        step(1, (), (3,))
        turn_some(1)

        def steady(s, carry):
            step(s, (), ())

            turn_some(s)
            return carry

        lax.fori_loop(2, steps, steady, 0)
        @pl.when(main)
        def _():
            up_copy.start()
            own_up.start()

        for sub in range(2):
            total = terms[rows_of(z, sub), :]
            for ch in range(4):
                rs_copy(ch, steps - 1, sub, 2).wait_recv()
                total = total + rs_in[ch, steps - 1, sub].astype(F32)
            outb[pl.ds(sub * rows, rows), :] = total.astype(BF16)
        out_copy.start()
        own_out.start()

        def rs_sent(s, carry):
            for sub in range(2):
                for ch in range(3):
                    rs_copy(ch, s, sub, 2).wait_send()

                @pl.when(s > 0)
                def _():
                    rs_copy(3, s, sub, 2).wait_send()

            return carry

        lax.fori_loop(0, steps, rs_sent, 0)
        out_copy.wait_send()
        own_out.wait()

    @pl.when(main)
    def _():
        rows_copy.wait_send()
        down_copy(left, 0, 0, 1).wait_send()
        down_copy(right, 1, 1, 1).wait_send()
        for d in range(2):
            for k in range(2):
                down_copy(x, k, d, 0).wait_send()
        for k, xs in enumerate((x, left, right, far)):
            down_across(xs, k, True).wait_send()

        def sent(i, carry):
            y_copy(i, True).wait_send()
            for k in range(2):
                x_copy(x, k, i, k * per_col + i, True).wait_send()
                x_copy(x, k, i, k * per_col + i, False).wait_send()

                @pl.when(i % 2 == 0)
                def _():
                    x_copy(left, k, i, relay_slot(k, i), True).wait_send()

                @pl.when(i % 2 == 1)
                def _():
                    x_copy(right, k, i, relay_slot(k, i), False).wait_send()

            return carry

        lax.fori_loop(0, per_col, sent, 0)
        dn_copy.wait_send()
        up_copy.wait_send()
        own_dn = pltpu.make_async_copy(half_of(dn, par, hid), dn_ref, l_sem.at[0])
        own_dn.wait()
        own_up.wait()

    @pl.when(apart)
    def _():
        dnt_copy.wait_send()
        ht_copy.wait_send()

    @pl.when(agent)
    def _():
        loads[3].wait()
        dn_copy.wait_recv()
        up_copy.wait_recv()

    @pl.when(c == 0)
    def _():
        out_copy.wait_recv()

    @pl.when(agent)
    def _():
        def scattered(j, carry):
            scatter_copy(j).wait_send()
            return carry

        lax.fori_loop(0, per_col, scattered, 0)


def result_kernel(*refs):
    sources, results, buffers, (in_sem, out_sem) = refs[:3], refs[3:6], refs[6:9], refs[9:]
    reads, writes = [], []
    for k in range(3):
        size = sources[k].shape[0] // 2 // 16 * 16
        for part, sl in enumerate((pl.ds(0, size), pl.ds(size, sources[k].shape[0] - size))):
            reads.append(pltpu.make_async_copy(sources[k].at[sl], buffers[k].at[sl], in_sem.at[k, part]))
            writes.append(pltpu.make_async_copy(buffers[k].at[sl], results[k].at[sl], out_sem.at[k, part]))
    for read in reads:
        read.start()
    for read, write in zip(reads, writes):
        read.wait()
        write.start()
    for write in writes:
        write.wait()


def solution(mesh):
    nz, nx = mesh.shape["fs"] // 2, mesh.shape["tp"]

    def shards(tokens, up_master, down_master, norm_gain):
        rows = up_master.shape[0]
        hid, dcols = down_master.shape
        count, width = tokens.shape
        feat, wide = 2 * rows, 2 * hid
        steps = nz // 4
        per_col = nz // nx
        dma = pltpu.SemaphoreType.DMA
        any_space = pl.BlockSpec(memory_space=pltpu.HBM)
        results = pl.pallas_call(
            functools.partial(kernel, nz, nx),
            out_shape=(
                jax.ShapeDtypeStruct((rows, count), BF16),
                jax.ShapeDtypeStruct((hid, width), BF16),
                jax.ShapeDtypeStruct((hid, width), BF16),
            ),
            in_specs=[any_space] * 4,
            out_specs=(any_space,) * 3,
            scratch_shapes=[
                pltpu.VMEM((count, width), BF16),
                pltpu.VMEM(up_master.shape, F32),
                pltpu.VMEM(down_master.shape, F32),
                pltpu.VMEM((1, rows), F32),
                pltpu.VMEM(up_master.shape, BF16),
                pltpu.VMEM(up_master.shape, BF16),
                pltpu.VMEM((width, wide), BF16),
                pltpu.VMEM((wide, width), BF16),
                pltpu.VMEM((count, width), BF16),
                pltpu.VMEM((width, wide), BF16),
                pltpu.VMEM((wide, width), BF16),
                pltpu.VMEM((count, wide), F32),
                pltpu.VMEM((wide, count), BF16),
                pltpu.VMEM((width, count), F32),
                pltpu.VMEM((4, steps, 2, rows, count), BF16),
                pltpu.VMEM((4, steps, 2, rows, count), BF16),
                pltpu.VMEM((feat, count), BF16),
                dma((4,)),
                dma((1,)),
                dma((1,)),
                dma((4,)),
                dma((4,)),
                dma((per_col,)),
                dma((per_col,)),
                dma((per_col,)),
                dma((per_col,)),
                dma((2, 3 * per_col)),
                dma((2, 3 * per_col)),
                dma((2, 2, 2)),
                dma((2, 2, 2)),
                dma((4, steps, 2)),
                dma((4, steps, 2)),
                dma((5,)),
                dma((5,)),
                dma((3,)),
            ],
            compiler_params=pltpu.CompilerParams(
                collective_id=0, has_side_effects=True, vmem_limit_bytes=60 * 1024 * 1024
            ),
        )(tokens, up_master, down_master, norm_gain[None])
        out_t, up_t, down = pl.pallas_call(
            result_kernel,
            out_shape=tuple(jax.ShapeDtypeStruct(r.shape, r.dtype) for r in results),
            in_specs=[any_space] * 3,
            out_specs=(any_space,) * 3,
            scratch_shapes=[pltpu.VMEM(r.shape, r.dtype) for r in results] + [dma((3, 2)), dma((3, 2))],
            compiler_params=pltpu.CompilerParams(vmem_limit_bytes=60 * 1024 * 1024),
        )(*results)
        return out_t.T, up_t.T, down

    return jax.shard_map(
        shards,
        mesh=mesh,
        in_specs=(P(("grp", "tp"), None), P("fs", "tp"), P("fs", "tp"), P("fs")),
        out_specs=(P(("grp", "tp"), "fs"), P("grp", "fs"), P(("grp", "fs"), None)),
        check_vma=False,
    )
```

profile of v0, /device:TPU:33, one launch (start us, length us, event | category | flops | bytes accessed | tf_op | source)
XLA Modules:
  0.0 128.9 jit_solution(944065262975086195)
XLA Ops:
  0.6 125.6 %shard_map.67 = (bf16[48,256]{1,0:T(8,128)(2,1)}, bf16[192,3072]{1,0:T(8,128)(2,1)}, bf16[192,3072]{1,0:T(8,128)(2,1)}) custom-call(bf16[256,3072]{1,0:T(8,128)(2,1)} %tok_hbm.1, f32[48,3072]{1,0:T(8,128)} %upm_hbm.1, f32[192,768]{1,0:T(8,128)} %dnm_hbm.1, f32[1,48]{1,0:T(1,128)} %bitcast.3), custom_call_target="tpu_custom_call" | custom-call | tf_op jit(solution)/shard_map/pallas_call | solution.py:493
  126.3 2.6 %shard_map.68 = (bf16[48,256]{1,0:T(8,128)(2,1)}, bf16[192,3072]{1,0:T(8,128)(2,1)}, bf16[192,3072]{1,0:T(8,128)(2,1)}) custom-call(bf16[48,256]{1,0:T(8,128)(2,1)} %get-tuple-element.9.refs_0_, bf16[192,3072]{1,0:T(8,128)(2,1)} %get-tuple-element.10.refs_1_, bf16[192,3072]{1,0:T(8,128)(2,1)} %get-tuple-element.11.refs_2_), custom_call_target="tpu_custom_call" | custom-call | tf_op jit(solution)/shard_map/pallas_call | solution.py:543
where the time goes:
time: 129 us
  Pallas kernels  128 us (99%)
    pallas_call x1, Pallas kernels, shards(): pl.pallas_call(functools.partial(kernel, nz, nx), out_shape=(jax.ShapeDty...  126 us
    pallas_call x1, Pallas kernels, shards(): pl.pallas_call(result_kernel, out_shape=tuple((jax.ShapeDtypeStruct(r.sha...  2.6 us

commit v1 on v0

--- a/solution.py
+++ b/solution.py
@@ -223,8 +223,9 @@
         own_dn = pltpu.make_async_copy(half_of(dn, par, hid), dn_ref, l_sem.at[0])
 
         def ordered(s):
-            near_first = jnp.where(s % 2 == 0, per_col - 1 - s // 2, s // 2)
-            return jnp.where(quarter == nx - 1, near_first, (s + 1) % per_col)
+            away = (s + 1) // 2
+            near_first = (z // nx + per_col + jnp.where(s % 2 == 1, away, -away)) % per_col
+            return jnp.where(quarter < nx // 2, (s + 1) % per_col, near_first)
 
         chunk = nx * feat
         acc[...] = jnp.zeros_like(acc)
@@ -244,7 +245,6 @@
             y_copy(i, False).wait_recv()
             x_copy(x, 1, i, per_col + i, True).start()
             x_copy(x, 1, i, per_col + i, False).start()
-            relay(0, i)
 
         def complete(i):
             for k in range(2):
@@ -271,7 +271,8 @@
 
             at_lag(s, 0, arrived)
             at_lag(s, 2, crossed)
-            at_lag(s, 4, lambda i: relay(1, i))
+            at_lag(s, 3, lambda i: relay(0, i))
+            at_lag(s, 5, lambda i: relay(1, i))
 
             @pl.when(s == per_col)
             def _():
@@ -285,10 +286,10 @@
                 def _():
                     dnt_copy.start()
 
-            at_lag(s, 5, complete)
-            return carry
-
-        lax.fori_loop(0, per_col + 5, gather_up, 0)
+            at_lag(s, 7, complete)
+            return carry
+
+        lax.fori_loop(0, per_col + 7, gather_up, 0)
 
         ht[...] = jnp.square(jnp.maximum(acc[...], 0.0)).T.astype(BF16)
 

time: 129 us -> 122 us (0.946)
  Pallas kernels: 128 us -> 121 us
    pallas_call x1, Pallas kernels: 126 us -> 118 us  [shards(): pl.pallas_call(functools.partial(kernel, nz, nx), out_shape=(jax.ShapeDty...]
where the time goes in v1:
time: 122 us; the launch traced here: 121 us
  Pallas kernels  121 us (99%)
    pallas_call x1, Pallas kernels, shards(): pl.pallas_call(functools.partial(kernel, nz, nx), out_shape=(jax.ShapeDty...  118 us
    pallas_call x1, Pallas kernels, shards(): pl.pallas_call(result_kernel, out_shape=tuple((jax.ShapeDtypeStruct(r.sha...  2.6 us

profile of v1, /device:TPU:33, one launch (start us, length us, event | category | flops | bytes accessed | tf_op | source)
XLA Modules:
  0.0 121.3 jit_solution(6628222240772573671)
XLA Ops:
  0.6 118.1 %shard_map.67 = (bf16[48,256]{1,0:T(8,128)(2,1)}, bf16[192,3072]{1,0:T(8,128)(2,1)}, bf16[192,3072]{1,0:T(8,128)(2,1)}) custom-call(bf16[256,3072]{1,0:T(8,128)(2,1)} %tok_hbm.1, f32[48,3072]{1,0:T(8,128)} %upm_hbm.1, f32[192,768]{1,0:T(8,128)} %dnm_hbm.1, f32[1,48]{1,0:T(1,128)} %bitcast.3), custom_call_target="tpu_custom_call" | custom-call | tf_op jit(solution)/shard_map/pallas_call | solution.py:494
  118.7 2.6 %shard_map.68 = (bf16[48,256]{1,0:T(8,128)(2,1)}, bf16[192,3072]{1,0:T(8,128)(2,1)}, bf16[192,3072]{1,0:T(8,128)(2,1)}) custom-call(bf16[48,256]{1,0:T(8,128)(2,1)} %get-tuple-element.9.refs_0_, bf16[192,3072]{1,0:T(8,128)(2,1)} %get-tuple-element.10.refs_1_, bf16[192,3072]{1,0:T(8,128)(2,1)} %get-tuple-element.11.refs_2_), custom_call_target="tpu_custom_call" | custom-call | tf_op jit(solution)/shard_map/pallas_call | solution.py:544

commit v2 on v1

--- a/solution.py
+++ b/solution.py
@@ -108,11 +108,19 @@
     peers = jnp.where(main, 5, 1 + per_col) + jnp.where(adds, 4, 0)
     pl.semaphore_wait(barrier, peers)
 
-    rows_copy = remote(stage, slots, xa_send.at[0], xa_recv.at[0], dev(g, z, 1 - par, (x + shift) % nx))
+    pieces = 4
+    per_piece = per_col // pieces
+
+    def rows_copy(k):
+        sl = pl.ds(k * per_piece * wide, per_piece * wide)
+        return remote(
+            stage.at[:, sl], slots.at[:, sl], xa_send.at[k], xa_recv.at[k], dev(g, z, 1 - par, (x + shift) % nx)
+        )
 
     @pl.when(main)
     def _():
-        rows_copy.start()
+        for k in range(pieces):
+            rows_copy(k).start()
 
     def scatter_copy(j):
         part = slots.at[:, pl.ds(pl.multiple_of(j * wide, 128), wide)]
@@ -122,13 +130,10 @@
 
     @pl.when(agent)
     def _():
-        rows_copy.wait_recv()
-
-        def scatter(k, carry):
-            scatter_copy(k).start()
-            return carry
-
-        lax.fori_loop(0, per_col, scatter, 0)
+        for k in range(pieces):
+            rows_copy(k).wait_recv()
+            for j in range(per_piece):
+                scatter_copy(k * per_piece + j).start()
 
     def to_mate(src, dst, k):
         return remote(src, dst, o_send.at[k], o_recv.at[k], dev(g, z, 1 - c, x))
@@ -269,12 +274,7 @@
                 down_copy(far, 1, 1, 1).wait_recv()
                 down_across(far, 3, True).start()
 
-            at_lag(s, 0, arrived)
-            at_lag(s, 2, crossed)
-            at_lag(s, 3, lambda i: relay(0, i))
-            at_lag(s, 5, lambda i: relay(1, i))
-
-            @pl.when(s == per_col)
+            @pl.when(s == 5)
             def _():
                 for k, xs in enumerate((x, left, right, far)):
                     down_across(xs, k, False).wait_recv()
@@ -285,6 +285,11 @@
                 @pl.when(apart)
                 def _():
                     dnt_copy.start()
+
+            at_lag(s, 0, arrived)
+            at_lag(s, 2, crossed)
+            at_lag(s, 3, lambda i: relay(0, i))
+            at_lag(s, 5, lambda i: relay(1, i))
 
             at_lag(s, 7, complete)
             return carry
@@ -406,7 +411,8 @@
 
     @pl.when(main)
     def _():
-        rows_copy.wait_send()
+        for k in range(pieces):
+            rows_copy(k).wait_send()
         down_copy(left, 0, 0, 1).wait_send()
         down_copy(right, 1, 1, 1).wait_send()
         for d in range(2):
@@ -519,8 +525,8 @@
                 pltpu.VMEM((4, steps, 2, rows, count), BF16),
                 pltpu.VMEM((feat, count), BF16),
                 dma((4,)),
-                dma((1,)),
-                dma((1,)),
+                dma((4,)),
+                dma((4,)),
                 dma((4,)),
                 dma((4,)),
                 dma((per_col,)),

time: 122 us -> 120 us (0.984)
  Pallas kernels: 121 us -> 119 us
    pallas_call x1, Pallas kernels: 118 us -> 116 us  [shards(): pl.pallas_call(functools.partial(kernel, nz, nx), out_shape=(jax.ShapeDty...]
where the time goes in v2:
time: 120 us; the launch traced here: 119 us
  Pallas kernels  119 us (99%)
    pallas_call x1, Pallas kernels, shards(): pl.pallas_call(functools.partial(kernel, nz, nx), out_shape=(jax.ShapeDty...  116 us
    pallas_call x1, Pallas kernels, shards(): pl.pallas_call(result_kernel, out_shape=tuple((jax.ShapeDtypeStruct(r.sha...  2.6 us

profile of v2, /device:TPU:33, one launch (start us, length us, event | category | flops | bytes accessed | tf_op | source)
XLA Modules:
  0.0 119.4 jit_solution(2100551146165925469)
XLA Ops:
  0.6 116.2 %shard_map.67 = (bf16[48,256]{1,0:T(8,128)(2,1)}, bf16[192,3072]{1,0:T(8,128)(2,1)}, bf16[192,3072]{1,0:T(8,128)(2,1)}) custom-call(bf16[256,3072]{1,0:T(8,128)(2,1)} %tok_hbm.1, f32[48,3072]{1,0:T(8,128)} %upm_hbm.1, f32[192,768]{1,0:T(8,128)} %dnm_hbm.1, f32[1,48]{1,0:T(1,128)} %bitcast.3), custom_call_target="tpu_custom_call" | custom-call | tf_op jit(solution)/shard_map/pallas_call | solution.py:500
  116.8 2.6 %shard_map.68 = (bf16[48,256]{1,0:T(8,128)(2,1)}, bf16[192,3072]{1,0:T(8,128)(2,1)}, bf16[192,3072]{1,0:T(8,128)(2,1)}) custom-call(bf16[48,256]{1,0:T(8,128)(2,1)} %get-tuple-element.9.refs_0_, bf16[192,3072]{1,0:T(8,128)(2,1)} %get-tuple-element.10.refs_1_, bf16[192,3072]{1,0:T(8,128)(2,1)} %get-tuple-element.11.refs_2_), custom_call_target="tpu_custom_call" | custom-call | tf_op jit(solution)/shard_map/pallas_call | solution.py:550

commit v3 on v2

--- a/solution.py
+++ b/solution.py
@@ -336,10 +336,10 @@
         def rows_of(zt, sub):
             return pl.ds(pl.multiple_of(zt * feat + sub * rows, 16), rows)
 
-        def step(s, skip, first_of):
-            for sub in range(2):
-                for ch in (1, 2, 0, 3):
-                    if ch in skip:
+        def step(s, runs, first_of):
+            for pair in ((1, 2), (0, 3)):
+                for sub, ch in ((0, pair[0]), (0, pair[1]), (1, pair[0]), (1, pair[1])):
+                    if ch not in runs:
                         continue
                     sign, odd = chains[ch]
                     d = half - odd - 2 * s
@@ -367,14 +367,15 @@
             return carry
 
         steps = half // 2
-        step(0, (3,), (0, 1, 2))
+        step(0, (1, 2), (1, 2))
         lax.fori_loop(0, terms.shape[0] // tc, all_terms, 0)
+        step(0, (0,), (0,))
         turn_some(0)
-        step(1, (), (3,))
+        step(1, (0, 1, 2, 3), (3,))
         turn_some(1)
 
         def steady(s, carry):
-            step(s, (), ())
+            step(s, (0, 1, 2, 3), ())
 
             turn_some(s)
             return carry

time: 120 us -> 120 us (level)
  no operation moved by 1% of the time
where the time goes in v3:
time: 120 us
  Pallas kernels  120 us (100%)
    pallas_call x1, Pallas kernels, shards(): pl.pallas_call(functools.partial(kernel, nz, nx), out_shape=(jax.ShapeDty...  117 us
    pallas_call x1, Pallas kernels, shards(): pl.pallas_call(result_kernel, out_shape=tuple((jax.ShapeDtypeStruct(r.sha...  2.6 us

profile of v3, /device:TPU:33, one launch (start us, length us, event | category | flops | bytes accessed | tf_op | source)
XLA Modules:
  0.0 120.2 jit_solution(13928730855291927538)
XLA Ops:
  0.6 117.0 %shard_map.67 = (bf16[48,256]{1,0:T(8,128)(2,1)}, bf16[192,3072]{1,0:T(8,128)(2,1)}, bf16[192,3072]{1,0:T(8,128)(2,1)}) custom-call(bf16[256,3072]{1,0:T(8,128)(2,1)} %tok_hbm.1, f32[48,3072]{1,0:T(8,128)} %upm_hbm.1, f32[192,768]{1,0:T(8,128)} %dnm_hbm.1, f32[1,48]{1,0:T(1,128)} %bitcast.3), custom_call_target="tpu_custom_call" | custom-call | tf_op jit(solution)/shard_map/pallas_call | solution.py:501
  117.6 2.6 %shard_map.68 = (bf16[48,256]{1,0:T(8,128)(2,1)}, bf16[192,3072]{1,0:T(8,128)(2,1)}, bf16[192,3072]{1,0:T(8,128)(2,1)}) custom-call(bf16[48,256]{1,0:T(8,128)(2,1)} %get-tuple-element.9.refs_0_, bf16[192,3072]{1,0:T(8,128)(2,1)} %get-tuple-element.10.refs_1_, bf16[192,3072]{1,0:T(8,128)(2,1)} %get-tuple-element.11.refs_2_), custom_call_target="tpu_custom_call" | custom-call | tf_op jit(solution)/shard_map/pallas_call | solution.py:551

commit v4 on v2

--- a/solution.py
+++ b/solution.py
@@ -230,7 +230,8 @@
         def ordered(s):
             away = (s + 1) // 2
             near_first = (z // nx + per_col + jnp.where(s % 2 == 1, away, -away)) % per_col
-            return jnp.where(quarter < nx // 2, (s + 1) % per_col, near_first)
+            falling = (2 * per_col - 2 - s) % per_col
+            return jnp.where(quarter < nx // 2, (s + 1) % per_col, jnp.where(quarter < nx - 1, falling, near_first))
 
         chunk = nx * feat
         acc[...] = jnp.zeros_like(acc)

time: 120 us -> 120 us (level)
  no operation moved by 1% of the time
where the time goes in v4:
time: 120 us
  Pallas kernels  119 us (99%)
    pallas_call x1, Pallas kernels, shards(): pl.pallas_call(functools.partial(kernel, nz, nx), out_shape=(jax.ShapeDty...  116 us
    pallas_call x1, Pallas kernels, shards(): pl.pallas_call(result_kernel, out_shape=tuple((jax.ShapeDtypeStruct(r.sha...  2.6 us

profile of v4, /device:TPU:33, one launch (start us, length us, event | category | flops | bytes accessed | tf_op | source)
XLA Modules:
  0.0 119.5 jit_solution(9241043568889658483)
XLA Ops:
  0.6 116.3 %shard_map.67 = (bf16[48,256]{1,0:T(8,128)(2,1)}, bf16[192,3072]{1,0:T(8,128)(2,1)}, bf16[192,3072]{1,0:T(8,128)(2,1)}) custom-call(bf16[256,3072]{1,0:T(8,128)(2,1)} %tok_hbm.1, f32[48,3072]{1,0:T(8,128)} %upm_hbm.1, f32[192,768]{1,0:T(8,128)} %dnm_hbm.1, f32[1,48]{1,0:T(1,128)} %bitcast.3), custom_call_target="tpu_custom_call" | custom-call | tf_op jit(solution)/shard_map/pallas_call | solution.py:501
  116.9 2.6 %shard_map.68 = (bf16[48,256]{1,0:T(8,128)(2,1)}, bf16[192,3072]{1,0:T(8,128)(2,1)}, bf16[192,3072]{1,0:T(8,128)(2,1)}) custom-call(bf16[48,256]{1,0:T(8,128)(2,1)} %get-tuple-element.9.refs_0_, bf16[192,3072]{1,0:T(8,128)(2,1)} %get-tuple-element.10.refs_1_, bf16[192,3072]{1,0:T(8,128)(2,1)} %get-tuple-element.11.refs_2_), custom_call_target="tpu_custom_call" | custom-call | tf_op jit(solution)/shard_map/pallas_call | solution.py:551

commit v5 on v4

--- a/solution.py
+++ b/solution.py
@@ -77,6 +77,7 @@
         lax.fori_loop(0, per_col, greet_agent, 0)
         for to_x in (right, left):
             greet(dev(g, z, par, to_x))
+            greet(dev(other, z, 1 - par, to_x))
         greet(dev(g, z, 1 - par, x))
         greet(dev(other, z, 1 - par, x))
 
@@ -105,7 +106,7 @@
     def _():
         dn_part(par, x)[...] = dnm[...].astype(BF16)
 
-    peers = jnp.where(main, 5, 1 + per_col) + jnp.where(adds, 4, 0)
+    peers = jnp.where(main, 7, 1 + per_col) + jnp.where(adds, 4, 0)
     pl.semaphore_wait(barrier, peers)
 
     pieces = 4
@@ -171,6 +172,11 @@
         d = 0 if to_right else 1
         part = piece(xs, k, i)
         return remote(part, part, x_send.at[d, slot], x_recv.at[d, slot], dev(g, z, par, right if to_right else left))
+
+    def diagonal(i, to_right):
+        d = 0 if to_right else 1
+        part, slot = piece(x, 0, i), per_col + i
+        return remote(part, part, x_send.at[d, slot], x_recv.at[d, slot], dev(other, z, 1 - par, right if to_right else left))
 
     def y_copy(i, mine):
         part = piece(x, 0 if mine else 1, i)
@@ -246,11 +252,11 @@
             y_copy(i, True).start()
             x_copy(x, 0, i, i, True).start()
             x_copy(x, 0, i, i, False).start()
+            diagonal(i, True).start()
+            diagonal(i, False).start()
 
         def crossed(i):
             y_copy(i, False).wait_recv()
-            x_copy(x, 1, i, per_col + i, True).start()
-            x_copy(x, 1, i, per_col + i, False).start()
 
         def complete(i):
             for k in range(2):
@@ -290,12 +296,11 @@
             at_lag(s, 0, arrived)
             at_lag(s, 2, crossed)
             at_lag(s, 3, lambda i: relay(0, i))
-            at_lag(s, 5, lambda i: relay(1, i))
-
-            at_lag(s, 7, complete)
-            return carry
-
-        lax.fori_loop(0, per_col + 7, gather_up, 0)
+            at_lag(s, 3, lambda i: relay(1, i))
+            at_lag(s, 6, complete)
+            return carry
+
+        lax.fori_loop(0, per_col + 6, gather_up, 0)
 
         ht[...] = jnp.square(jnp.maximum(acc[...], 0.0)).T.astype(BF16)
 

time: 120 us -> 118 us (0.983)
    pallas_call x1, Pallas kernels: 116 us -> 115 us  [shards(): pl.pallas_call(functools.partial(kernel, nz, nx), out_shape=(jax.ShapeDty...]
where the time goes in v5:
time: 118 us
  Pallas kernels  118 us (100%)
    pallas_call x1, Pallas kernels, shards(): pl.pallas_call(functools.partial(kernel, nz, nx), out_shape=(jax.ShapeDty...  115 us
    pallas_call x1, Pallas kernels, shards(): pl.pallas_call(result_kernel, out_shape=tuple((jax.ShapeDtypeStruct(r.sha...  2.6 us

profile of v5, /device:TPU:33, one launch (start us, length us, event | category | flops | bytes accessed | tf_op | source)
XLA Modules:
  0.0 118.2 jit_solution(5706996082087061968)
XLA Ops:
  0.6 115.0 %shard_map.67 = (bf16[48,256]{1,0:T(8,128)(2,1)}, bf16[192,3072]{1,0:T(8,128)(2,1)}, bf16[192,3072]{1,0:T(8,128)(2,1)}) custom-call(bf16[256,3072]{1,0:T(8,128)(2,1)} %tok_hbm.1, f32[48,3072]{1,0:T(8,128)} %upm_hbm.1, f32[192,768]{1,0:T(8,128)} %dnm_hbm.1, f32[1,48]{1,0:T(1,128)} %bitcast.3), custom_call_target="tpu_custom_call" | custom-call | tf_op jit(solution)/shard_map/pallas_call | solution.py:506
  115.6 2.6 %shard_map.68 = (bf16[48,256]{1,0:T(8,128)(2,1)}, bf16[192,3072]{1,0:T(8,128)(2,1)}, bf16[192,3072]{1,0:T(8,128)(2,1)}) custom-call(bf16[48,256]{1,0:T(8,128)(2,1)} %get-tuple-element.9.refs_0_, bf16[192,3072]{1,0:T(8,128)(2,1)} %get-tuple-element.10.refs_1_, bf16[192,3072]{1,0:T(8,128)(2,1)} %get-tuple-element.11.refs_2_), custom_call_target="tpu_custom_call" | custom-call | tf_op jit(solution)/shard_map/pallas_call | solution.py:556
